TPU v7x, 32 devices: a whole 2x2x4 slice. The times are simulated.
32 devices in a mesh: sp: 8 (over z, y), tp: 4 (over x, core).
Axes of the slice: x: 2, y: 2, z: 4, core: 2. Of those that a mesh axis runs over, the one named last changes fastest.
Arguments:
- tokens: bfloat16 [3072, 2048], P('sp', 'tp'), may hold values from -6 to 6
- norm_gain: float32 [2048], replicated, may hold values from 0.1 to 1.9
- w_query_down: bfloat16 [2048, 512], replicated, may hold values from -0.125 to 0.125
- query_gain: float32 [512], replicated, may hold values from 0.1 to 1.9
- w_query_up: bfloat16 [512, 1536], P(None, 'tp'), may hold values from -0.25 to 0.25
- w_latent_down: bfloat16 [2048, 256], replicated, may hold values from -0.125 to 0.125
- latent_gain: float32 [256], replicated, may hold values from 0.1 to 1.9
- w_rotary_key: bfloat16 [2048, 32], replicated, may hold values from -0.125 to 0.125
- w_latent_up: bfloat16 [256, 2048], P(None, 'tp'), may hold values from -0.375 to 0.375
- query_head_gain: float32 [96], replicated, may hold values from 0.1 to 1.9
- key_head_gain: float32 [96], replicated, may hold values from 0.1 to 1.9
- w_pool_in: bfloat16 [2048, 1024], P(None, 'tp'), may hold values from -0.125 to 0.125
- w_pool_mix: bfloat16 [4, 256, 256], P('tp'), may hold values from -0.375 to 0.375
- pool_scale: float32 [1024], P('tp'), may hold values from 0.1 to 1.9
- w_attn_out: bfloat16 [1024, 2048], P('tp'), may hold values from -12 to 12
- w_pool_out: bfloat16 [1024, 2048], P('tp'), may hold values from -0.5 to 0.5
- w_gate_attn: bfloat16 [2048, 2048], P(None, 'tp'), may hold values from -0.125 to 0.125
- w_gate_pool: bfloat16 [2048, 2048], P(None, 'tp'), may hold values from -0.125 to 0.125
Outputs:
- mixed: bfloat16 [3072, 2048], P('sp', 'tp')
All inputs are finite; a program needn't handle non-finite values.
Results may differ from a plain program's by a relative error of at most 0.02.
Values may be sent and summed in bfloat16 or wider, within the bound.
A program may use at most 128 MiB of HBM per device.

v0:
```python
import functools
import math
import types

import jax
import numpy as np
import jax.numpy as jnp
from jax import lax
from jax.experimental import pallas as pl
from jax.experimental.pallas import tpu as pltpu
from jax.sharding import PartitionSpec as P

NOPE = 64
ROPE = 32
TURN = ROPE // 2
WIDTH = NOPE + ROPE
VALUE_DIM = 64
POOL_GROUPS = 4
POOL_GROUP = 256
LANES = 128
HALO = 16

eps = 1e-06
theta = 10000.0
f32 = jnp.float32
bf = jnp.bfloat16
MESH = pl.DeviceIdType.MESH
NT = (((1,), (1,)), ((), ()))


def flip(index, offset):
    bit = 1
    while bit <= offset:
        if offset & bit:
            index = index + bit - 2 * bit * ((index // bit) % 2)
        bit *= 2
    return index


def mm(a, b):
    return jnp.dot(a, b, preferred_element_type=f32)


def mm_nt(a, b):
    return lax.dot_general(a, b, NT, preferred_element_type=f32)


def phase(name):
    pass


def kernel(n, m, names, *refs):
    r = types.SimpleNamespace(**dict(zip(names, refs)))
    s = lax.axis_index("sp")
    t = lax.axis_index("tp")
    rows, cols = r.out.shape
    pairs = n // 2
    p = s // 2
    y = s % 2
    half = rows // 2
    across = flip(s, 1)
    twin = flip(t, 1)
    core = t % 2
    other = (s + n + 2 * y - 1) % n
    heads = r.queries.shape[0]
    rank = r.lat.shape[3]
    hc = cols // 2
    tiles = rows // LANES

    nearest = [
        sorted(range(pairs), key=lambda gap: (abs((q + gap) % pairs - q), gap)) for q in range(pairs)
    ]

    def gap_of(i):
        gap = jnp.int32(0)
        for q in range(pairs):
            if isinstance(i, int):
                mine_of = nearest[q][i]
            else:
                mine_of = jnp.int32(0)
                for k in range(1, pairs):
                    mine_of = mine_of + jnp.where(i == k, nearest[q][k], 0)
            gap = gap + jnp.where(p == q, mine_of, 0)
        return gap

    def same_parity(i):
        return ((p + i) % pairs) * 2 + y

    phase("barrier")
    barrier = pltpu.get_barrier_semaphore()
    peers = [(s, flip(t, off)) for off in range(1, m)]
    peers += [(same_parity(i), t) for i in range(1, pairs)]
    peers += [(across, t), (other, t)]
    for peer in peers:
        pl.semaphore_signal(barrier, inc=1, device_id=peer, device_id_type=MESH)

    def columns(block):
        return pl.ds(pl.multiple_of(block * cols, cols), cols)

    fetch = {}

    def take(name, src, dst, slot):
        copy = pltpu.make_async_copy(src, dst, r.local_sem.at[slot])
        copy.start()
        fetch.setdefault(name, []).append(copy)

    def have(*wanted):
        for name in wanted:
            for copy in fetch.pop(name, ()):
                copy.wait()

    take("tokens", r.h_tokens, r.tok.at[0], 0)
    mine = pl.ds(pl.multiple_of(t * cols, cols), cols)
    take("norm_gain", r.h_norm_gain, r.norm_gain, 1)
    take("w_latent_down", r.h_w_latent_down.at[mine, :], r.w_latent_down, 2)
    take("w_rotary", r.h_w_rotary.at[:, mine], r.w_rotary, 3)
    slot = 4
    for name in ("w_query_down", "w_gate_attn", "w_gate_pool", "w_pool_in"):
        for off in range(m):
            rows_of = pl.ds(pl.multiple_of(flip(t, off) * cols, cols), cols)
            place = pl.ds(off * cols, cols)
            source = getattr(r, "h_" + name).at[rows_of, :]
            take(name, source, getattr(r, name).at[place, :], slot)
        slot += 1
    for name in (
        "freqs",
        "w_query_up",
        "w_latent_up",
        "gain_q",
        "gain_k",
        "latent_gain",
        "query_gain",
        "w_pool_mix",
        "pool_scale",
    ):
        take("small", getattr(r, "h_" + name), getattr(r, name), slot)
    depth = r.wa.shape[2]
    for j in range(heads // 2):
        take("wa", r.h_attn_out.at[pl.ds(j * depth, depth), columns(t)], r.wa.at[j, 0], slot + 1)
    for o in range(m // 2):
        take("wp", r.h_pool_out.at[:, columns(flip(t, 2 * o))], r.wp.at[o, 0], slot + 2)

    def ready(off, start, size):
        base = flip(t, off) * cols + start
        raw = r.tok[off, :, start : start + size].astype(f32)
        gain = r.norm_gain[:, pl.ds(pl.multiple_of(base, hc), size)]
        spot = slice(off * cols + start, off * cols + start + size)
        r.scaled[:rows, spot] = (raw * gain).astype(bf)
        return jnp.sum(raw * raw, axis=-1, keepdims=True)

    def ready_edge(off):
        raw = r.edge[off].astype(f32)
        gain = r.norm_gain[:, columns(flip(t, off))]
        r.scaled[rows:, off * cols : (off + 1) * cols] = (raw * gain).astype(bf)
        return jnp.sum(raw * raw, axis=-1, keepdims=True)

    lane = lax.broadcasted_iota(jnp.int32, (1, LANES), 1)
    have("tokens", "norm_gain")
    squares = ready(0, 0, cols)
    have("w_latent_down", "w_rotary")
    part = mm(r.scaled[:rows, :cols], r.w_latent_down[...])
    side = mm_nt(r.scaled[:rows, :cols], r.w_rotary[...])
    side = jnp.concatenate([side, jnp.zeros((rows, LANES - ROPE), f32)], axis=1)
    side = jnp.where(lane == ROPE, squares, side)
    for e in range(2):
        r.sum_own[e, :, :rank] = part[e * half : (e + 1) * half]
        r.sum_own[e, :, rank:] = side[e * half : (e + 1) * half]
    pl.semaphore_wait(barrier, len(peers))

    def remote(src, dst, recv, peer):
        return pltpu.make_async_remote_copy(
            src_ref=src,
            dst_ref=dst,
            send_sem=r.sent,
            recv_sem=recv,
            device_id=peer,
            device_id_type=MESH,
        )

    def push(view, sem, off, least=1, most=m // 2):
        bit = most
        while bit >= least:
            if off == 0 or bit < (off & -off):
                slot = off ^ bit
                remote(view(off), view(slot), sem.at[slot - 1], (s, flip(t, bit))).start()
            bit //= 2

    def arrive(view, sem, off):
        remote(view(0), view(off), sem.at[off - 1], (s, t)).wait_recv()
        push(view, sem, off)

    def drain(view, sem):
        for slot in range(1, m):
            remote(view(0), view(slot), sem.at[slot - 1], (s, t)).wait_send()

    phase("push0")
    sum_copy = remote(r.sum_own.at[1 - core], r.sum_in, r.sum_sem, (s, twin))
    sum_copy.start()
    parts = 4
    width = cols // parts

    def tok_view(c):
        return lambda off: r.tok.at[off, :, pl.ds(c * width, width)]

    push(tok_view(0), r.tok_sem.at[0], 0, 2)
    downward = remote(
        r.tok.at[0, pl.ds(rows - HALO, HALO), :],
        r.edge.at[0, pl.ds(0, HALO), :],
        r.halo_sem.at[0],
        ((s + 1) % n, t),
    )
    upward = remote(
        r.tok.at[0, pl.ds(0, HALO), :],
        r.edge.at[0, pl.ds(HALO, HALO), :],
        r.halo_sem.at[1],
        ((s + n - 1) % n, t),
    )
    downward.start()
    upward.start()
    for c in range(parts):
        push(tok_view(c), r.tok_sem.at[c], 0, 1, 1)

    pair_copies = []
    for o in range(m // 2):
        pair_copies.append(
            remote(
                r.h_pool_out.at[:, columns(flip(twin, 2 * o))],
                r.wp.at[o, 1],
                r.wp_sem.at[o],
                (s, twin),
            )
        )
    for j in range(heads // 2):
        pair_copies.append(
            remote(
                r.h_attn_out.at[pl.ds(j * depth, depth), columns(twin)],
                r.wa.at[j, 1],
                r.wt_sem.at[j],
                (s, twin),
            )
        )
    for copy in pair_copies:
        copy.start()
    chunks = heads // 2
    share = chunks // 2

    def shared(half_of):
        return pl.ds(half_of * share, share)

    far_copies = []
    for off in range(2, m):
        for j in range(share):
            piece = y * share + j
            far_copies.append(
                remote(
                    r.h_attn_out.at[
                        pl.ds(pl.multiple_of(piece * depth, depth), depth), columns(flip(t, off))
                    ],
                    r.wa.at[piece, off],
                    r.wa_sem.at[off - 2, j],
                    (s, flip(t, off)),
                )
            )

    def over(off, j):
        piece = y * share + j
        return remote(
            r.wa.at[piece, off],
            r.wa.at[piece, off],
            r.wf_sem.at[off - 2, j],
            (across, t),
        )

    phase("own")

    def partial(off, w, start, size):
        spot = slice(off * cols + start, off * cols + start + size)
        return mm(r.scaled[:rows, spot], w[spot, :])

    def edge_view(off):
        return r.edge.at[off]

    wides = (
        ("w_query_down", r.acc_q, r.w_query_down),
        ("w_gate_attn", r.acc_ga, r.w_gate_attn),
        ("w_gate_pool", r.acc_gp, r.w_gate_pool),
        ("w_pool_in", r.acc_p, r.w_pool_in),
    )
    first = list(range(max(m // 2, 1)))
    later = list(range(max(m // 2, 1), m))
    for name, acc, w in wides[:1]:
        have(name)
        acc[...] = partial(0, w, 0, cols)

    phase("sum_pair")
    sum_copy.wait_recv()
    total = r.sum_own[core] + r.sum_in[...]
    side = jnp.concatenate([total[:, rank:], jnp.zeros((rank - half, LANES), f32)], axis=0).T
    row = lax.broadcasted_iota(jnp.int32, (TURN, rank), 0)
    levels = side[ROPE : ROPE + 1]
    coarse = levels.astype(bf).astype(f32)
    tail = jnp.where(row == 0, coarse, jnp.where(row == 1, levels - coarse, 0.0))
    r.sum_main[...] = total[:, :rank]
    r.sum_side[...] = side[: ROPE + 8]
    r.far_out[:half, :] = total[:, :rank].astype(bf)
    r.far_out[half : half + ROPE, :] = side[:ROPE].astype(bf)
    r.far_out[half + ROPE :, :] = tail.astype(bf)
    far_sums = []
    for off in range(2, m, 2):
        far_sums.append(
            remote(
                r.far_out,
                r.far_in.at[off // 2 - 1],
                r.fs_sem.at[off // 2 - 1],
                (s, flip(t, off)),
            )
        )
        far_sums[-1].start()
    for c in range(1, parts - 1):
        push(tok_view(c), r.tok_sem.at[c], 0, 2)

    phase("own2")
    for name, acc, w in wides[1:]:
        have(name)
        acc[...] = partial(0, w, 0, cols)
    phase("edge")
    downward.wait_recv()
    upward.wait_recv()
    push(edge_view, r.edge_sem, 0)
    push(tok_view(parts - 1), r.tok_sem.at[parts - 1], 0, 2)
    phase("own3")
    squares_edge = ready_edge(0)
    for off in first[1:]:
        for c in range(parts):
            arrive(tok_view(c), r.tok_sem.at[c], off)
        squares += ready(off, 0, cols)
        for name, acc, w in wides:
            acc[...] += partial(off, w, 0, cols)
    for off in first[1:]:
        arrive(edge_view, r.edge_sem, off)
        squares_edge += ready_edge(off)
    span = len(first) * cols
    r.acc_e[...] = mm(r.scaled[rows:, :span], r.w_pool_in[:span, :])

    phase("tables")
    have("small")
    freqs = jnp.concatenate([r.freqs[...]] * tiles, axis=1)
    along = lax.broadcasted_iota(jnp.int32, (ROPE, rows), 1)

    def table(k, carry):
        source = ((p + k // 2) % pairs) * 2 + (y + k) % 2
        angles = (source * rows + along[:TURN]).astype(f32) * freqs
        r.cosine[k] = jnp.cos(angles)
        r.sine[k] = jnp.sin(angles)
        return carry

    lax.fori_loop(0, n, table, 0)

    low = lane < NOPE
    spare = jnp.zeros((1, LANES - WIDTH), f32)
    turning = (lane >= NOPE) & (lane < WIDTH)

    def partner(values):
        swapped = jnp.where(
            lane < NOPE + TURN,
            pltpu.roll(values, LANES - TURN, 1),
            pltpu.roll(values, TURN, 1),
        )
        return jnp.where(turning, swapped, 0.0)

    gain_q = jnp.concatenate([r.gain_q[...], spare], axis=1)
    gain_q = gain_q * (WIDTH**-0.5 * math.log2(math.e))
    gain_q = jnp.broadcast_to(gain_q, (8, LANES))
    gain_p = partner(gain_q)
    side = jnp.zeros((LANES - WIDTH, rows), f32)
    cosine = jnp.concatenate([jnp.ones((NOPE, rows), f32), r.cosine[0], r.cosine[0], side], axis=0)
    sine = jnp.concatenate([jnp.zeros((NOPE, rows), f32), -r.sine[0], r.sine[0], side], axis=0)
    r.turn_q[0] = cosine.T * gain_q[:1]
    r.turn_q[1] = sine.T * gain_p[:1]
    gain_k = jnp.concatenate([r.gain_k[...], spare], axis=1)
    gain_k = jnp.broadcast_to(gain_k, (LANES, LANES)).T
    r.gain_rows[...] = jnp.concatenate([gain_k] * tiles, axis=1)

    for h in range(heads):
        up = r.w_query_up[:, h * WIDTH : (h + 1) * WIDTH].astype(f32)
        up = jnp.concatenate([up, jnp.zeros((up.shape[0], LANES - WIDTH), f32)], axis=1)
        r.up_q[:, h * LANES : (h + 1) * LANES] = up.astype(bf)
        r.up_q[:, (heads + h) * LANES : (heads + h + 1) * LANES] = partner(up).astype(bf)
    r.up_k[...] = r.w_latent_up[...].astype(f32).T.astype(bf)
    for e in range(2):
        for h in range(heads):
            r.keys[e, h, WIDTH:, :] = jnp.zeros((LANES - WIDTH, 2 * rows), bf)
            row = lax.broadcasted_iota(jnp.int32, (LANES - VALUE_DIM, 2 * rows), 0)
            r.values[e, h, VALUE_DIM:, :] = jnp.where(row == 0, 1.0, 0.0).astype(bf)
    r.attn_acc[...] = jnp.zeros_like(r.attn_acc)
    groups = r.w_pool_mix.shape[0]
    column = lax.broadcasted_iota(jnp.int32, (rows, rows + LANES), 1)
    before = (column >= rows) & (column < rows + HALO)
    column = jnp.where(before, column - rows - HALO, jnp.where(column < rows, column, column - HALO))
    apart = column - lax.broadcasted_iota(jnp.int32, (rows, rows + LANES), 0)
    place = s * rows + column
    exists = (place >= 0) & (place < rows * n)

    def reach_of(j):
        group = t * groups + j
        reach = jnp.int32(0)
        for i in range(POOL_GROUPS):
            reach = reach + jnp.where(group == i, 2**i, 0)
        return reach

    for j in range(groups):
        reach = reach_of(j)
        inside = exists & (apart >= -reach) & (apart <= reach - 1)
        r.band[j] = jnp.where(inside, 1.0, 0.0).astype(bf)
    pool = r.padded.shape[1]
    r.padded[pl.ds(rows + 2 * HALO, LANES - 2 * HALO), :] = jnp.zeros(
        (LANES - 2 * HALO, pool), bf
    )

    def rms(values, gain, width):
        mean = jnp.sum(values * values, axis=-1, keepdims=True) / width
        return values * lax.rsqrt(mean + eps) * gain

    phase("sum_far")
    main = r.sum_main[...]
    side = r.sum_side[:ROPE, :]
    levels = r.sum_side[ROPE : ROPE + 1, :]
    for i, copy in enumerate(far_sums):
        copy.wait_recv()
        main += r.far_in[i, :half, :].astype(f32)
        side += r.far_in[i, half : half + ROPE, :].astype(f32)
        tail = r.far_in[i, half + ROPE :, :].astype(f32)
        levels += tail[:1] + tail[1:2]
    level_row = lax.rsqrt(levels / (cols * m) + eps)
    level_column = jnp.broadcast_to(level_row, (LANES, rank)).T[:half, :1]
    latent = (main * level_column).astype(bf).astype(f32)
    r.lat[0, core, :half, :] = rms(latent, r.latent_gain[...], rank).astype(bf)
    r.lat[0, core, half:, :] = (side * level_row).astype(bf)

    near_copy = remote(
        r.lat.at[0, core], r.lat.at[1, core], r.main_sem.at[0], (across, t)
    )
    near_copy.start()
    for i in range(1, pairs):
        gap = (pairs - gap_of(i)) % pairs
        remote(
            r.lat.at[0, core],
            r.lat.at[2 * gap, core],
            r.main_sem.at[2 * gap - 1],
            (same_parity(pairs - gap), t),
        ).start()

    def main_wait(k):
        remote(
            r.lat.at[0, core], r.lat.at[k, core], r.main_sem.at[k - 1], (s, t)
        ).wait_recv()

    def to_across(k):
        return remote(
            r.lat.at[k, core], r.lat.at[k + 1, core], r.main_sem.at[k], (across, t)
        )

    def to_twin(k):
        return remote(
            r.lat.at[k, core], r.lat.at[k, core], r.pair_sem.at[k], (s, twin)
        )

    def twin_wait(k):
        remote(
            r.lat.at[k, core], r.lat.at[k, 1 - core], r.pair_sem.at[k], (s, twin)
        ).wait_recv()

    to_twin(0).start()

    def gather_tokens(h):
        total = 0.0
        for c in range(h * parts // 2, (h + 1) * parts // 2):
            for off in later:
                arrive(tok_view(c), r.tok_sem.at[c], off)
        if h == 1:
            for copy in far_copies:
                copy.start()
        for off in later:
            total += ready(off, h * hc, hc)
        return total

    def prepare(k, slot, e):
        latent = jnp.concatenate([r.lat[k, 0, :half, :], r.lat[k, 1, :half, :]], axis=0)

        def turns(part):
            got = r.lat[k, part, half:, :].astype(f32)
            return jnp.concatenate([got, jnp.zeros((ROPE, rows - rank), f32)], axis=1)

        whole = jnp.where(along < half, turns(0), pltpu.roll(turns(1), half, 1))
        x1 = whole[:TURN]
        x2 = whole[TURN:]
        shared_sum = jnp.sum(x1 * x1 + x2 * x2, axis=0, keepdims=True)
        x1 = x1 * r.gain_rows[NOPE : NOPE + TURN, :]
        x2 = x2 * r.gain_rows[NOPE + TURN : WIDTH, :]
        cosine = r.cosine[k]
        sine = r.sine[k]
        turn1 = x1 * cosine - x2 * sine
        turn2 = x1 * sine + x2 * cosine
        both = mm_nt(r.up_k[...], latent)
        spot = slice(e * rows, (e + 1) * rows)
        for h in range(heads):
            plain = both[h * LANES : h * LANES + NOPE].astype(bf).astype(f32)
            value = both[h * LANES + NOPE : (h + 1) * LANES].astype(bf)
            total = jnp.sum(plain * plain, axis=0, keepdims=True)
            level = lax.rsqrt((total + shared_sum) / WIDTH + eps)
            r.keys[slot, h, :NOPE, spot] = (plain * r.gain_rows[:NOPE, :] * level).astype(bf)
            r.keys[slot, h, NOPE : NOPE + TURN, spot] = (turn1 * level).astype(bf)
            r.keys[slot, h, NOPE + TURN : WIDTH, spot] = (turn2 * level).astype(bf)
            r.values[slot, h, :VALUE_DIM, spot] = value

    def attend(slot, h):
        scores = mm(r.queries[h], r.keys[slot, h])
        weighted = mm_nt(jnp.exp2(scores).astype(bf), r.values[slot, h])
        r.attn_acc[h] += weighted

    def forward(i):
        ahead = 2 * gap_of(i)
        main_wait(ahead)
        to_across(ahead).start()
        to_twin(ahead).start()

    def gather(i):
        now = 2 * gap_of(i)
        main_wait(now + 1)
        to_twin(now + 1).start()

    phase("later0")
    squares += gather_tokens(0)
    for name, acc, w in wides:
        total = acc[...]
        for off in later:
            total += partial(off, w, 0, hc)
        acc[...] = total

    phase("prep0")
    twin_wait(0)
    prepare(0, 0, 0)
    phase("wait_ahead")

    @pl.when(core == 1)
    def _():
        forward(1)

    phase("later1")
    for off in later:
        arrive(edge_view, r.edge_sem, off)
        squares_edge += ready_edge(off)
    r.acc_e[...] += mm(r.scaled[rows:, span:], r.w_pool_in[span:, :])
    squares += gather_tokens(1)
    scale = lax.rsqrt(squares / (cols * m) + eps)

    def finish(acc, w):
        total = acc[...]
        for off in later:
            total += partial(off, w, hc, hc)
        return total

    phase("pool_input")
    scale_edge = lax.rsqrt(squares_edge / (cols * m) + eps)
    r.padded[:rows, :] = (finish(r.acc_p, r.w_pool_in) * scale).astype(bf)
    r.padded[rows : rows + 2 * HALO, :] = (r.acc_e[...] * scale_edge).astype(bf)
    phase("pool")
    position = s * rows + lax.broadcasted_iota(jnp.int32, (rows, 1), 0)
    for j in range(groups):
        reach = reach_of(j)
        part = slice(j * POOL_GROUP, (j + 1) * POOL_GROUP)
        total = mm(r.band[j], r.padded[:, part])
        start = jnp.maximum(position - reach, 0)
        stop = jnp.minimum(position + reach, rows * n)
        count = (stop - start).astype(f32)
        own = r.padded[:rows, part].astype(f32)
        mixed = (total / count - own).astype(bf)
        r.prow[0, :, part] = (mm(mixed, r.w_pool_mix[j]) * r.pool_scale[:, part]).astype(bf)
    prow_copy = remote(r.prow.at[0], r.prow.at[1], r.pr_sem, (s, twin))
    prow_copy.start()
    phase("across0")
    gather(0)
    phase("ahead1")

    @pl.when(core == 0)
    def _():
        forward(1)

    phase("query")
    query_latent = (finish(r.acc_q, r.w_query_down) * scale).astype(bf).astype(f32)
    query_normed = rms(query_latent, r.query_gain[...], query_latent.shape[1]).astype(bf)
    query_raw = mm(query_normed, r.up_q[...])
    for h in range(heads):
        raw = query_raw[:, h * LANES : (h + 1) * LANES].astype(bf).astype(f32)
        swapped = query_raw[:, (heads + h) * LANES : (heads + h + 1) * LANES].astype(bf).astype(f32)
        mean = jnp.sum(raw * raw, axis=-1, keepdims=True) / WIDTH
        turned = raw * r.turn_q[0] + swapped * r.turn_q[1]
        r.queries[h] = (turned * lax.rsqrt(mean + eps)).astype(bf)

    phase("pool_out")
    prow_copy.wait_recv()
    have("wp")
    for o in range(m // 2):
        pair_copies[o].wait_recv()
    part_copies = []
    pool_rows = jnp.concatenate([r.prow[0], r.prow[1]], axis=1)
    for o in range(m // 2 - 1, -1, -1):
        weights = jnp.concatenate([r.wp[o, 0], r.wp[o, 1]], axis=0)
        branch = mm(pool_rows, weights)
        if o:
            r.psend[o - 1] = branch.astype(bf)
            copy = remote(
                r.psend.at[o - 1],
                r.precv.at[o - 1],
                r.pp_sem.at[o - 1],
                (s, flip(t, 2 * o)),
            )
            copy.start()
            part_copies.append(copy)
        else:
            r.acc_b[...] = branch

    phase("ahead2")
    if pairs > 2:
        forward(2)
    twin_wait(1)
    phase("pair0")
    prepare(1, 0, 1)
    for h in range(heads):
        attend(0, h)
    phase("across1")
    gather(1)
    phase("ahead3")
    if pairs > 3:
        forward(3)

    def relay():
        for off in range(2, m):
            for j in range(share):
                far_copies[(off - 2) * share + j].wait_recv()
                over(off, j).start()

    phase("steps")

    def step(i, carry):
        now = 2 * gap_of(i)

        @pl.when(i + 3 < pairs)
        def _():
            forward(i + 3)

        @pl.when(i == max(pairs - 4, 1))
        def _():
            relay()

        twin_wait(now)
        twin_wait(now + 1)
        prepare(now, i % 2, 0)
        prepare(now + 1, i % 2, 1)
        for h in range(chunks):
            attend(i % 2, h)
        gather(i + 1)
        for h in range(chunks, heads):
            attend(i % 2, h)
        return carry

    lax.fori_loop(1, pairs - 1, step, 0)

    phase("last_wait")
    i = pairs - 1
    now = 2 * gap_of(i)
    twin_wait(now)
    twin_wait(now + 1)
    phase("last_attend")
    prepare(now, i % 2, 0)
    prepare(now + 1, i % 2, 1)

    def rows_view(j):
        return lambda off: r.arows.at[j, off]

    for j in range(chunks):
        for h in (2 * j, 2 * j + 1):
            attend(i % 2, h)
        even = r.attn_acc[2 * j]
        odd = r.attn_acc[2 * j + 1]
        even = even / even[:, VALUE_DIM : VALUE_DIM + 1]
        odd = odd / odd[:, VALUE_DIM : VALUE_DIM + 1]
        r.arows[j, 0] = jnp.where(low, even, pltpu.roll(odd, VALUE_DIM, 1)).astype(bf)
        push(rows_view(j), r.ar_sem.at[j], 0)

    phase("gates")
    r.acc_ga[...] = lax.logistic(finish(r.acc_ga, r.w_gate_attn) * scale)
    r.acc_gp[...] = lax.logistic(finish(r.acc_gp, r.w_gate_pool) * scale)

    phase("pool_sum")
    branch = r.acc_b[...]
    for copy in part_copies:
        copy.wait_recv()
    for o in range(1, m // 2):
        branch += r.precv[o - 1].astype(f32)
    r.acc_gp[...] *= branch

    phase("w_wait")
    have("wa")
    for j in range(chunks):
        pair_copies[m // 2 + j].wait_recv()
    for off in range(2, m):
        for j in range(share):
            remote(
                r.wa.at[0, off],
                r.wa.at[(1 - y) * share + j, off],
                r.wf_sem.at[off - 2, j],
                (across, t),
            ).wait_recv()
    total = None
    for j in range(chunks):
        phase("rows%d" % j)
        for off in range(1, m):
            arrive(rows_view(j), r.ar_sem.at[j], off)
        phase("out%d" % j)
        left = jnp.concatenate([r.arows[j, off] for off in range(m)], axis=1)
        branch = mm(left, r.wa[j].reshape(m * depth, cols))
        total = branch if total is None else total + branch
    r.out[...] = (r.acc_ga[...] * total + r.acc_gp[...]).astype(bf)

    phase("drain")
    for c in range(parts):
        drain(tok_view(c), r.tok_sem.at[c])
    drain(edge_view, r.edge_sem)
    for j in range(chunks):
        drain(rows_view(j), r.ar_sem.at[j])
    for copy in pair_copies + far_copies + part_copies + far_sums + [sum_copy, prow_copy, downward, upward]:
        copy.wait_send()
    for off in range(2, m):
        for j in range(share):
            over(off, j).wait_send()
    for i in range(pairs):
        remote(r.lat.at[0, core], r.lat.at[0, core], r.main_sem.at[0], (s, t)).wait_send()
    for k in range(n):
        to_twin(k).wait_send()
        if k and k % 2 == 0:
            to_across(k).wait_send()
    phase(None)


def body(
    n,
    m,
    tokens,
    norm_gain,
    w_query_down,
    query_gain,
    w_query_up,
    w_latent_down,
    latent_gain,
    w_rotary_key,
    w_latent_up,
    query_head_gain,
    key_head_gain,
    w_pool_in,
    w_pool_mix,
    pool_scale,
    w_attn_out,
    w_pool_out,
    w_gate_attn,
    w_gate_pool,
):
    rows, cols = tokens.shape
    heads = w_query_up.shape[1] // WIDTH
    rank = w_latent_down.shape[1]
    qrank = w_query_down.shape[1]
    pool = w_pool_in.shape[1]
    groups = w_pool_mix.shape[0]
    chunks = heads // 2
    share = chunks // 2
    depth = w_attn_out.shape[0] // chunks
    freqs = np.repeat(theta ** (-np.arange(TURN) / TURN)[:, None], LANES, axis=1)
    dma = pltpu.SemaphoreType.DMA
    inputs = {
        "h_tokens": tokens,
        "h_norm_gain": norm_gain[None, :],
        "h_w_query_down": w_query_down,
        "h_query_gain": query_gain[None, :],
        "h_w_query_up": w_query_up,
        "h_w_latent_down": w_latent_down,
        "h_latent_gain": latent_gain[None, :],
        "h_w_rotary": w_rotary_key.T,
        "h_w_latent_up": w_latent_up,
        "h_gain_q": query_head_gain[None, :],
        "h_gain_k": key_head_gain[None, :],
        "h_w_pool_in": w_pool_in,
        "h_w_pool_mix": w_pool_mix,
        "h_pool_scale": pool_scale[None, :],
        "h_attn_out": w_attn_out,
        "h_pool_out": w_pool_out,
        "h_w_gate_attn": w_gate_attn,
        "h_w_gate_pool": w_gate_pool,
        "h_freqs": jnp.asarray(freqs, f32),
    }
    scratch = {}
    for name, value in inputs.items():
        if name not in ("h_tokens", "h_attn_out", "h_pool_out"):
            scratch[name[2:]] = pltpu.VMEM(value.shape, value.dtype)
    scratch["w_latent_down"] = pltpu.VMEM((cols, rank), bf)
    scratch["w_rotary"] = pltpu.VMEM((ROPE, cols), bf)
    scratch.update(
        tok=pltpu.VMEM((m, rows, cols), bf),
        scaled=pltpu.VMEM((rows + 2 * HALO, m * cols), bf),
        edge=pltpu.VMEM((m, 2 * HALO, cols), bf),
        acc_p=pltpu.VMEM((rows, pool), f32),
        acc_e=pltpu.VMEM((2 * HALO, pool), f32),
        wa=pltpu.VMEM((chunks, m, depth, cols), bf),
        wp=pltpu.VMEM((m // 2, 2, pool, cols), bf),
        acc_q=pltpu.VMEM((rows, qrank), f32),
        sum_own=pltpu.VMEM((2, rows // 2, rank + LANES), f32),
        sum_in=pltpu.VMEM((rows // 2, rank + LANES), f32),
        sum_main=pltpu.VMEM((rows // 2, rank), f32),
        sum_side=pltpu.VMEM((ROPE + 8, rank), f32),
        far_out=pltpu.VMEM((rows // 2 + ROPE + TURN, rank), bf),
        far_in=pltpu.VMEM((m // 2 - 1, rows // 2 + ROPE + TURN, rank), bf),
        acc_ga=pltpu.VMEM((rows, cols), f32),
        acc_gp=pltpu.VMEM((rows, cols), f32),
        acc_b=pltpu.VMEM((rows, cols), f32),
        cosine=pltpu.VMEM((n, TURN, rows), f32),
        sine=pltpu.VMEM((n, TURN, rows), f32),
        turn_q=pltpu.VMEM((2, rows, LANES), f32),
        gain_rows=pltpu.VMEM((LANES, rows), f32),
        up_q=pltpu.VMEM((qrank, 2 * heads * LANES), bf),
        up_k=pltpu.VMEM((heads * LANES, rank), bf),
        queries=pltpu.VMEM((heads, rows, LANES), bf),
        lat=pltpu.VMEM((n, 2, rows // 2 + ROPE, rank), bf),
        keys=pltpu.VMEM((2, heads, LANES, 2 * rows), bf),
        values=pltpu.VMEM((2, heads, LANES, 2 * rows), bf),
        attn_acc=pltpu.VMEM((heads, rows, LANES), f32),
        band=pltpu.VMEM((groups, rows, rows + LANES), bf),
        padded=pltpu.VMEM((rows + LANES, pool), bf),
        prow=pltpu.VMEM((2, rows, pool), bf),
        psend=pltpu.VMEM((m // 2 - 1, rows, cols), bf),
        precv=pltpu.VMEM((m // 2 - 1, rows, cols), bf),
        arows=pltpu.VMEM((chunks, m, rows, LANES), bf),
        local_sem=dma((11,)),
        sent=dma,
        tok_sem=dma((4, m - 1)),
        edge_sem=dma((m - 1,)),
        sum_sem=dma,
        fs_sem=dma((m // 2 - 1,)),
        wp_sem=dma((m // 2,)),
        wt_sem=dma((chunks,)),
        wa_sem=dma((m - 2, share)),
        wf_sem=dma((m - 2, share)),
        ar_sem=dma((chunks, m - 1)),
        pr_sem=dma,
        pp_sem=dma((m // 2 - 1,)),
        halo_sem=dma((2,)),
        main_sem=dma((n - 1,)),
        pair_sem=dma((n,)),
    )
    names = list(inputs) + ["out"] + list(scratch)
    return pl.pallas_call(
        functools.partial(kernel, n, m, names),
        out_shape=pltpu.VMEM((rows, cols), bf),
        in_specs=[pl.BlockSpec(memory_space=pl.ANY)] * len(inputs),
        out_specs=pl.BlockSpec(memory_space=pltpu.VMEM),
        scratch_shapes=list(scratch.values()),
        compiler_params=pltpu.CompilerParams(collective_id=0, has_side_effects=True),
    )(*inputs.values())


def solution(mesh):
    placed = (
        P("sp", "tp"),
        P(),
        P(),
        P(),
        P(None, "tp"),
        P(),
        P(),
        P(),
        P(None, "tp"),
        P(),
        P(),
        P(None, "tp"),
        P("tp", None, None),
        P("tp"),
        P("tp", None),
        P("tp", None),
        P(None, "tp"),
        P(None, "tp"),
    )
    held = functools.partial(body, mesh.shape["sp"], mesh.shape["tp"])
    return jax.shard_map(held, mesh=mesh, in_specs=placed, out_specs=P("sp", "tp"), check_vma=False)
```

profile of v0, /device:TPU:1, one launch (start us, length us, event | category | flops | bytes accessed | tf_op | source)
XLA Modules:
  0.0 43.8 jit_solution(4231885994690361726)
XLA Ops:
  0.0 43.1 %shard_map.181 = bf16[384,512]{1,0:T(8,128)(2,1)S(1)} custom-call(bf16[384,512]{1,0:T(8,128)(2,1)} %refs_0_.1, f32[1,2048]{1,0:T(1,128)} %bitcast.8, bf16[2048,512]{1,0:T(8,128)(2,1)} %refs_2_.1, f32[1,512]{1,0:T(1,128)} %bitcast.9, bf16[512,384]{1,0:T(8,128)(2,1)} %refs_4_.1, bf16[2048,256]{1,0:T(8,128)(2,1)} %refs_5_.1, f32[1,256]{1,0:T(1,128)} %bitcast.10, ...), custom_call_target="tpu_custom_call" | custom-call | tf_op jit(solution)/shard_map/pallas_call | solution.py:859
  43.1 0.7 %copy.21 = bf16[384,512]{1,0:T(8,128)(2,1)} copy(bf16[384,512]{1,0:T(8,128)(2,1)S(1)} %shard_map.181) | data formatting | bytes 786432
where the time goes:
time: 44 us; the launch traced here: 43.8 us
  Pallas kernels  43.1 us (98%)
  local copies, waits for them, and re-layouts  0.75 us (2%)
    pallas_call x1, Pallas kernels, body(): pl.pallas_call(functools.partial(kernel, n, m, names), out_shape=pltpu.VM...  43.1 us

commit v1 on v0

--- a/solution.py
+++ b/solution.py
@@ -18,7 +18,7 @@
 POOL_GROUPS = 4
 POOL_GROUP = 256
 LANES = 128
-HALO = 16
+HALO = 8
 
 eps = 1e-06
 theta = 10000.0
@@ -247,29 +247,33 @@
     def shared(half_of):
         return pl.ds(half_of * share, share)
 
+    beside = flip(s, 2)
+    level = p % 2
+    slab = depth // 2
+
+    def slab_rows(start, which):
+        return pl.ds(pl.multiple_of(start + which * slab, slab), slab)
+
     far_copies = []
     for off in range(2, m):
         for j in range(share):
             piece = y * share + j
             far_copies.append(
                 remote(
-                    r.h_attn_out.at[
-                        pl.ds(pl.multiple_of(piece * depth, depth), depth), columns(flip(t, off))
-                    ],
-                    r.wa.at[piece, off],
+                    r.h_attn_out.at[slab_rows(piece * depth, level), columns(flip(t, off))],
+                    r.wa.at[piece, off, slab_rows(0, level)],
                     r.wa_sem.at[off - 2, j],
                     (s, flip(t, off)),
                 )
             )
 
+    def along_line(off, j):
+        part = r.wa.at[y * share + j, off, slab_rows(0, level)]
+        return remote(part, part, r.wz_sem.at[off - 2, j], (beside, t))
+
     def over(off, j):
-        piece = y * share + j
-        return remote(
-            r.wa.at[piece, off],
-            r.wa.at[piece, off],
-            r.wf_sem.at[off - 2, j],
-            (across, t),
-        )
+        piece = r.wa.at[y * share + j, off]
+        return remote(piece, piece, r.wf_sem.at[off - 2, j], (across, t))
 
     phase("own")
 
@@ -342,8 +346,80 @@
     span = len(first) * cols
     r.acc_e[...] = mm(r.scaled[rows:, :span], r.w_pool_in[:span, :])
 
+    have("small")
+
+    def rms(values, gain, width):
+        mean = jnp.sum(values * values, axis=-1, keepdims=True) / width
+        return values * lax.rsqrt(mean + eps) * gain
+
+    phase("sum_far")
+    main = r.sum_main[...]
+    side = r.sum_side[:ROPE, :]
+    levels = r.sum_side[ROPE : ROPE + 1, :]
+    for i, copy in enumerate(far_sums):
+        copy.wait_recv()
+        main += r.far_in[i, :half, :].astype(f32)
+        side += r.far_in[i, half : half + ROPE, :].astype(f32)
+        tail = r.far_in[i, half + ROPE :, :].astype(f32)
+        levels += tail[:1] + tail[1:2]
+    level_row = lax.rsqrt(levels / (cols * m) + eps)
+    level_column = jnp.broadcast_to(level_row, (LANES, rank)).T[:half, :1]
+    latent = (main * level_column).astype(bf).astype(f32)
+    r.lat[0, core, :half, :] = rms(latent, r.latent_gain[...], rank).astype(bf)
+    r.lat[0, core, half:, :] = (side * level_row).astype(bf)
+
+    near_copy = remote(
+        r.lat.at[0, core], r.lat.at[1, core], r.main_sem.at[0], (across, t)
+    )
+    near_copy.start()
+
+    def send(i):
+        gap = (pairs - gap_of(i)) % pairs
+        remote(
+            r.lat.at[0, core],
+            r.lat.at[2 * gap, core],
+            r.main_sem.at[2 * gap - 1],
+            (same_parity(pairs - gap), t),
+        ).start()
+
+    inner = (p > 0) & (p < pairs - 1)
+    outer = jnp.logical_not(inner)
+    head = p == 0
+    tail_end = p == pairs - 1
+
+    def only(condition, act, i):
+        if i < pairs:
+
+            @pl.when(condition)
+            def _():
+                act(i)
+
+    send(1)
+    only(inner, send, 2)
+
+    def main_wait(k):
+        remote(
+            r.lat.at[0, core], r.lat.at[k, core], r.main_sem.at[k - 1], (s, t)
+        ).wait_recv()
+
+    def to_across(k):
+        return remote(
+            r.lat.at[k, core], r.lat.at[k + 1, core], r.main_sem.at[k], (across, t)
+        )
+
+    def to_twin(k):
+        return remote(
+            r.lat.at[k, core], r.lat.at[k, core], r.pair_sem.at[k], (s, twin)
+        )
+
+    def twin_wait(k):
+        remote(
+            r.lat.at[k, core], r.lat.at[k, 1 - core], r.pair_sem.at[k], (s, twin)
+        ).wait_recv()
+
+    to_twin(0).start()
+
     phase("tables")
-    have("small")
     freqs = jnp.concatenate([r.freqs[...]] * tiles, axis=1)
     along = lax.broadcasted_iota(jnp.int32, (ROPE, rows), 1)
 
@@ -417,69 +493,22 @@
         (LANES - 2 * HALO, pool), bf
     )
 
-    def rms(values, gain, width):
-        mean = jnp.sum(values * values, axis=-1, keepdims=True) / width
-        return values * lax.rsqrt(mean + eps) * gain
-
-    phase("sum_far")
-    main = r.sum_main[...]
-    side = r.sum_side[:ROPE, :]
-    levels = r.sum_side[ROPE : ROPE + 1, :]
-    for i, copy in enumerate(far_sums):
-        copy.wait_recv()
-        main += r.far_in[i, :half, :].astype(f32)
-        side += r.far_in[i, half : half + ROPE, :].astype(f32)
-        tail = r.far_in[i, half + ROPE :, :].astype(f32)
-        levels += tail[:1] + tail[1:2]
-    level_row = lax.rsqrt(levels / (cols * m) + eps)
-    level_column = jnp.broadcast_to(level_row, (LANES, rank)).T[:half, :1]
-    latent = (main * level_column).astype(bf).astype(f32)
-    r.lat[0, core, :half, :] = rms(latent, r.latent_gain[...], rank).astype(bf)
-    r.lat[0, core, half:, :] = (side * level_row).astype(bf)
-
-    near_copy = remote(
-        r.lat.at[0, core], r.lat.at[1, core], r.main_sem.at[0], (across, t)
-    )
-    near_copy.start()
-    for i in range(1, pairs):
-        gap = (pairs - gap_of(i)) % pairs
-        remote(
-            r.lat.at[0, core],
-            r.lat.at[2 * gap, core],
-            r.main_sem.at[2 * gap - 1],
-            (same_parity(pairs - gap), t),
-        ).start()
-
-    def main_wait(k):
-        remote(
-            r.lat.at[0, core], r.lat.at[k, core], r.main_sem.at[k - 1], (s, t)
-        ).wait_recv()
-
-    def to_across(k):
-        return remote(
-            r.lat.at[k, core], r.lat.at[k + 1, core], r.main_sem.at[k], (across, t)
-        )
-
-    def to_twin(k):
-        return remote(
-            r.lat.at[k, core], r.lat.at[k, core], r.pair_sem.at[k], (s, twin)
-        )
-
-    def twin_wait(k):
-        remote(
-            r.lat.at[k, core], r.lat.at[k, 1 - core], r.pair_sem.at[k], (s, twin)
-        ).wait_recv()
-
-    to_twin(0).start()
-
     def gather_tokens(h):
         total = 0.0
         for c in range(h * parts // 2, (h + 1) * parts // 2):
             for off in later:
                 arrive(tok_view(c), r.tok_sem.at[c], off)
-        if h == 1:
-            for copy in far_copies:
-                copy.start()
+            if c == 0:
+                only(head, send, 2)
+                only(jnp.logical_not(head), send, 3)
+            if c == parts // 2:
+                only(head, send, 3)
+                only(tail_end, send, 2)
+                for i in range(4, pairs):
+                    send(i)
+                for copy in far_copies:
+                    copy.start()
+                only(inner, forward, 2)
         for off in later:
             total += ready(off, h * hc, hc)
         return total
@@ -540,12 +569,10 @@
     phase("prep0")
     twin_wait(0)
     prepare(0, 0, 0)
-    phase("wait_ahead")
-
-    @pl.when(core == 1)
-    def _():
-        forward(1)
-
+    phase("across0")
+    gather(0)
+    phase("ahead1")
+    forward(1)
     phase("later1")
     for off in later:
         arrive(edge_view, r.edge_sem, off)
@@ -578,14 +605,6 @@
         r.prow[0, :, part] = (mm(mixed, r.w_pool_mix[j]) * r.pool_scale[:, part]).astype(bf)
     prow_copy = remote(r.prow.at[0], r.prow.at[1], r.pr_sem, (s, twin))
     prow_copy.start()
-    phase("across0")
-    gather(0)
-    phase("ahead1")
-
-    @pl.when(core == 0)
-    def _():
-        forward(1)
-
     phase("query")
     query_latent = (finish(r.acc_q, r.w_query_down) * scale).astype(bf).astype(f32)
     query_normed = rms(query_latent, r.query_gain[...], query_latent.shape[1]).astype(bf)
@@ -597,6 +616,17 @@
         turned = raw * r.turn_q[0] + swapped * r.turn_q[1]
         r.queries[h] = (turned * lax.rsqrt(mean + eps)).astype(bf)
 
+    phase("ahead2")
+    only(outer, forward, 2)
+    only(jnp.logical_not(tail_end), forward, 3)
+    def relay_line():
+        for off in range(2, m):
+            for j in range(share):
+                far_copies[(off - 2) * share + j].wait_recv()
+                along_line(off, j).start()
+
+    phase("across1")
+    gather(1)
     phase("pool_out")
     prow_copy.wait_recv()
     have("wp")
@@ -620,24 +650,24 @@
         else:
             r.acc_b[...] = branch
 
-    phase("ahead2")
-    if pairs > 2:
-        forward(2)
+    phase("relay_line")
+    relay_line()
+    phase("pair0")
     twin_wait(1)
-    phase("pair0")
     prepare(1, 0, 1)
     for h in range(heads):
         attend(0, h)
-    phase("across1")
-    gather(1)
     phase("ahead3")
-    if pairs > 3:
-        forward(3)
-
+    only(tail_end, forward, 3)
     def relay():
         for off in range(2, m):
             for j in range(share):
-                far_copies[(off - 2) * share + j].wait_recv()
+                remote(
+                    r.wa.at[y * share + j, off, slab_rows(0, level)],
+                    r.wa.at[y * share + j, off, slab_rows(0, 1 - level)],
+                    r.wz_sem.at[off - 2, j],
+                    (beside, t),
+                ).wait_recv()
                 over(off, j).start()
 
     phase("steps")
@@ -648,10 +678,6 @@
         @pl.when(i + 3 < pairs)
         def _():
             forward(i + 3)
-
-        @pl.when(i == max(pairs - 4, 1))
-        def _():
-            relay()
 
         twin_wait(now)
         twin_wait(now + 1)
@@ -660,6 +686,11 @@
         for h in range(chunks):
             attend(i % 2, h)
         gather(i + 1)
+
+        @pl.when(i == pairs - 2)
+        def _():
+            relay()
+
         for h in range(chunks, heads):
             attend(i % 2, h)
         return carry
@@ -678,11 +709,12 @@
     def rows_view(j):
         return lambda off: r.arows.at[j, off]
 
-    for j in range(chunks):
-        for h in (2 * j, 2 * j + 1):
+    order = [y * share + j for j in range(share)] + [(1 - y) * share + j for j in range(share)]
+    for j, chunk in enumerate(order):
+        for h in (2 * chunk, 2 * chunk + 1):
             attend(i % 2, h)
-        even = r.attn_acc[2 * j]
-        odd = r.attn_acc[2 * j + 1]
+        even = r.attn_acc[2 * chunk]
+        odd = r.attn_acc[2 * chunk + 1]
         even = even / even[:, VALUE_DIM : VALUE_DIM + 1]
         odd = odd / odd[:, VALUE_DIM : VALUE_DIM + 1]
         r.arows[j, 0] = jnp.where(low, even, pltpu.roll(odd, VALUE_DIM, 1)).astype(bf)
@@ -704,23 +736,26 @@
     have("wa")
     for j in range(chunks):
         pair_copies[m // 2 + j].wait_recv()
-    for off in range(2, m):
-        for j in range(share):
-            remote(
-                r.wa.at[0, off],
-                r.wa.at[(1 - y) * share + j, off],
-                r.wf_sem.at[off - 2, j],
-                (across, t),
-            ).wait_recv()
     total = None
     for j in range(chunks):
         phase("rows%d" % j)
-        for off in range(1, m):
+        for off in range(1, m - 1):
             arrive(rows_view(j), r.ar_sem.at[j], off)
+        if j == share:
+            for off in range(2, m):
+                for k in range(share):
+                    remote(
+                        r.wa.at[0, off],
+                        r.wa.at[(1 - y) * share + k, off],
+                        r.wf_sem.at[off - 2, k],
+                        (across, t),
+                    ).wait_recv()
+        left = jnp.concatenate([r.arows[j, off] for off in range(m - 1)], axis=1)
+        branch = mm(left, r.wa[order[j], : m - 1].reshape((m - 1) * depth, cols))
+        total = branch if total is None else total + branch
+        arrive(rows_view(j), r.ar_sem.at[j], m - 1)
         phase("out%d" % j)
-        left = jnp.concatenate([r.arows[j, off] for off in range(m)], axis=1)
-        branch = mm(left, r.wa[j].reshape(m * depth, cols))
-        total = branch if total is None else total + branch
+        total += mm(r.arows[j, m - 1], r.wa[order[j], m - 1])
     r.out[...] = (r.acc_ga[...] * total + r.acc_gp[...]).astype(bf)
 
     phase("drain")
@@ -734,6 +769,7 @@
     for off in range(2, m):
         for j in range(share):
             over(off, j).wait_send()
+            along_line(off, j).wait_send()
     for i in range(pairs):
         remote(r.lat.at[0, core], r.lat.at[0, core], r.main_sem.at[0], (s, t)).wait_send()
     for k in range(n):
@@ -848,6 +884,7 @@
         wt_sem=dma((chunks,)),
         wa_sem=dma((m - 2, share)),
         wf_sem=dma((m - 2, share)),
+        wz_sem=dma((m - 2, share)),
         ar_sem=dma((chunks, m - 1)),
         pr_sem=dma,
         pp_sem=dma((m // 2 - 1,)),

time: 44 us -> 42.3 us (0.961)
  Pallas kernels: 43.1 us -> 41.4 us
    pallas_call x1, Pallas kernels: 43.1 us -> 41.4 us  [body(): pl.pallas_call(functools.partial(kernel, n, m, names), out_shape=pltpu.VM...]
where the time goes in v1:
time: 42.3 us; the launch traced here: 42.2 us
  Pallas kernels  41.4 us (98%)
  local copies, waits for them, and re-layouts  0.75 us (2%)
    pallas_call x1, Pallas kernels, body(): pl.pallas_call(functools.partial(kernel, n, m, names), out_shape=pltpu.VM...  41.4 us

profile of v1, /device:TPU:1, one launch (start us, length us, event | category | flops | bytes accessed | tf_op | source)
XLA Modules:
  0.0 42.2 jit_solution(10203210686919105486)
XLA Ops:
  0.0 41.4 %shard_map.181 = bf16[384,512]{1,0:T(8,128)(2,1)S(1)} custom-call(bf16[384,512]{1,0:T(8,128)(2,1)} %refs_0_.1, f32[1,2048]{1,0:T(1,128)} %bitcast.8, bf16[2048,512]{1,0:T(8,128)(2,1)} %refs_2_.1, f32[1,512]{1,0:T(1,128)} %bitcast.9, bf16[512,384]{1,0:T(8,128)(2,1)} %refs_4_.1, bf16[2048,256]{1,0:T(8,128)(2,1)} %refs_5_.1, f32[1,256]{1,0:T(1,128)} %bitcast.10, ...), custom_call_target="tpu_custom_call" | custom-call | tf_op jit(solution)/shard_map/pallas_call | solution.py:896
  41.5 0.7 %copy.21 = bf16[384,512]{1,0:T(8,128)(2,1)} copy(bf16[384,512]{1,0:T(8,128)(2,1)S(1)} %shard_map.181) | data formatting | bytes 786432

commit v2 on v1

--- a/solution.py
+++ b/solution.py
@@ -217,9 +217,6 @@
     )
     downward.start()
     upward.start()
-    for c in range(parts):
-        push(tok_view(c), r.tok_sem.at[c], 0, 1, 1)
-
     pair_copies = []
     for o in range(m // 2):
         pair_copies.append(
@@ -239,8 +236,6 @@
                 (s, twin),
             )
         )
-    for copy in pair_copies:
-        copy.start()
     chunks = heads // 2
     share = chunks // 2
 
@@ -322,6 +317,8 @@
         far_sums[-1].start()
     for c in range(1, parts - 1):
         push(tok_view(c), r.tok_sem.at[c], 0, 2)
+    for c in range(parts):
+        push(tok_view(c), r.tok_sem.at[c], 0, 1, 1)
 
     phase("own2")
     for name, acc, w in wides[1:]:
@@ -332,6 +329,8 @@
     upward.wait_recv()
     push(edge_view, r.edge_sem, 0)
     push(tok_view(parts - 1), r.tok_sem.at[parts - 1], 0, 2)
+    for copy in pair_copies:
+        copy.start()
     phase("own3")
     squares_edge = ready_edge(0)
     for off in first[1:]:
@@ -383,7 +382,6 @@
         ).start()
 
     inner = (p > 0) & (p < pairs - 1)
-    outer = jnp.logical_not(inner)
     head = p == 0
     tail_end = p == pairs - 1
 
@@ -587,6 +585,8 @@
             total += partial(off, w, hc, hc)
         return total
 
+    phase("head2")
+    only(head, forward, 2)
     phase("pool_input")
     scale_edge = lax.rsqrt(squares_edge / (cols * m) + eps)
     r.padded[:rows, :] = (finish(r.acc_p, r.w_pool_in) * scale).astype(bf)
@@ -617,7 +617,7 @@
         r.queries[h] = (turned * lax.rsqrt(mean + eps)).astype(bf)
 
     phase("ahead2")
-    only(outer, forward, 2)
+    only(tail_end, forward, 2)
     only(jnp.logical_not(tail_end), forward, 3)
     def relay_line():
         for off in range(2, m):

time: 42.3 us -> 42.3 us (level)
  no operation moved by 1% of the time
where the time goes in v2:
time: 42.3 us; the launch traced here: 42.2 us
  Pallas kernels  41.4 us (98%)
  local copies, waits for them, and re-layouts  0.75 us (2%)
    pallas_call x1, Pallas kernels, body(): pl.pallas_call(functools.partial(kernel, n, m, names), out_shape=pltpu.VM...  41.4 us

profile of v2, /device:TPU:1, one launch (start us, length us, event | category | flops | bytes accessed | tf_op | source)
XLA Modules:
  0.0 42.2 jit_solution(7912176769370679905)
XLA Ops:
  0.0 41.4 %shard_map.181 = bf16[384,512]{1,0:T(8,128)(2,1)S(1)} custom-call(bf16[384,512]{1,0:T(8,128)(2,1)} %refs_0_.1, f32[1,2048]{1,0:T(1,128)} %bitcast.8, bf16[2048,512]{1,0:T(8,128)(2,1)} %refs_2_.1, f32[1,512]{1,0:T(1,128)} %bitcast.9, bf16[512,384]{1,0:T(8,128)(2,1)} %refs_4_.1, bf16[2048,256]{1,0:T(8,128)(2,1)} %refs_5_.1, f32[1,256]{1,0:T(1,128)} %bitcast.10, ...), custom_call_target="tpu_custom_call" | custom-call | tf_op jit(solution)/shard_map/pallas_call | solution.py:896
  41.4 0.7 %copy.21 = bf16[384,512]{1,0:T(8,128)(2,1)} copy(bf16[384,512]{1,0:T(8,128)(2,1)S(1)} %shard_map.181) | data formatting | bytes 786432
